TPU v7x, 256 devices: a 4x2x16 block of a 4x16x16 slice. The times are simulated.
256 devices in a mesh: grp: 2 (over y), ep: 32 (over z, core), tp: 4 (over x).
Axes of the slice: x: 4, y: 2, z: 16, core: 2. Of those that a mesh axis runs over, the one named last changes fastest.
The devices are a block of a 4x16x16 slice.
Arguments:
- x_in: bfloat16 [4096, 2048], P(('grp', 'ep')), parts along dimension 0, may hold values from -6 to 6
- state: float32 [4096, 96, 128], P(('grp', 'ep'), 'tp'), parts along dimension 0, may hold values from -6 to 6
- routes: int32 [4096, 2], P(('grp', 'ep')), parts along dimension 0, may hold values from 0 to 63, as said below
- w_in: bfloat16 [2048, 1536], P(None, 'tp'), may hold values from -0.125 to 0.125
- decay_rate: float32 [96, 64], P('tp'), may hold values from 0.01 to 1
- frequency: float32 [96, 64], P('tp'), may hold values from 0 to 192
- log_step: float32 [96], P('tp'), may hold values from -3 to 0
- b_in: float32 [96, 16, 128], P('tp'), may hold values from -1.5 to 1.5
- c_out: float32 [96, 16, 128], P('tp'), may hold values from -0.5 to 0.5
- skip: float32 [1536], P('tp'), may hold values from -3 to 3
- w_out: bfloat16 [1536, 2048], P('tp'), may hold values from -0.15625 to 0.15625
- gain_mix: float32 [2048], replicated, may hold values from 0.1 to 1.9
- w_group: bfloat16 [2048, 4], replicated, may hold values from -0.0625 to 0.0625
- w_expert: bfloat16 [2048, 64], replicated, may hold values from -0.0625 to 0.0625
- w_gate: bfloat16 [64, 2048, 1024], P('ep', None, 'tp'), may hold values from -0.125 to 0.125
- w_up: bfloat16 [64, 2048, 1024], P('ep', None, 'tp'), may hold values from -0.125 to 0.125
- w_down: bfloat16 [64, 1024, 2048], P('ep', 'tp'), may hold values from -3 to 3
- gain_moe: float32 [2048], replicated, may hold values from 0.1 to 1.9
Outputs:
- layer_out: bfloat16 [4096, 2048], P(('grp', 'ep')), parts along dimension 0
- new_state: float32 [4096, 96, 128], P(('grp', 'ep'), 'tp'), parts along dimension 0
There are 2 independent parts, one for each index of `grp`. A program takes and returns all parts, laid end to end along the dimension named above; an argument that names none is the same for every part. Nothing has to cross between parts.
Inputs may be any that keep to these rules, and one draw needn't show every extreme that they name: `routes`: each row names two different experts of one group of 16 consecutive expert numbers. Within the rows of one index of ep (aligned blocks of 64 rows) no expert is named by more than 4 rows, and in every block some expert is named by exactly 4 rows.
All inputs are finite; a program needn't handle non-finite values.
Results may differ from a plain program's by a relative error of at most 0.015.
Values may be sent and summed in bfloat16 or wider, within the bound.
A program may use at most 64 MiB of HBM per device.

v0:
```python
import jax
import jax.numpy as jnp
from jax import lax
from jax.sharding import PartitionSpec as P

residual_scale = 8.0**0.25
norm_eps = 1e-05


def sent_to_all(x, axis):
    devices = lax.axis_size(axis)
    return lax.all_to_all(jnp.broadcast_to(x[None], (devices, *x.shape)), axis, 0, 0, tiled=True)


def taken_together(x, axis):
    everything = sent_to_all(x, axis)
    return jnp.sum(everything.astype(jnp.float32), axis=0)


def in_order(parts, dim):
    lengths = list(parts.shape[1:])
    lengths[dim] *= parts.shape[0]
    return jnp.moveaxis(parts, 0, dim).reshape(lengths)


def gather_directly(x, axis, dim):
    parts = sent_to_all(x, axis)
    return in_order(parts, dim)


def split_up(x, dim, devices):
    before, after = (x.shape[:dim], x.shape[dim + 1 :])
    return jnp.moveaxis(x.reshape(*before, devices, -1, *after), dim, 0)


def sent_and_summed(x, axis, dim):
    devices = lax.axis_size(axis)
    parts = lax.all_to_all(split_up(x, dim, devices), axis, 0, 0, tiled=True)
    return jnp.sum(parts.astype(jnp.float32), axis=0)


def normalize(values, gain):
    centre = jnp.mean(values, -1, keepdims=True)
    spread = jnp.mean(jnp.square(values - centre), -1, keepdims=True)
    return (values - centre) * lax.rsqrt(spread + norm_eps) * gain


def s5_advance(mix_input, state, decay_rate, frequency, log_step, b_in, c_out, skip):
    top_precision = lax.Precision.DEFAULT
    entries = decay_rate.shape[-1]
    group_count = decay_rate.shape[0]
    width = b_in.shape[1]
    seq_count = mix_input.shape[0]
    input_rows = mix_input.astype(jnp.float32).reshape(seq_count, group_count, width)
    step_size = jnp.exp(log_step)[:, None]
    lam_real = -decay_rate
    magnitude = jnp.exp(lam_real * step_size)
    angle_dt = frequency * step_size
    bar_real = magnitude * jnp.cos(angle_dt)
    bar_imag = magnitude * jnp.sin(angle_dt)
    minus_real = bar_real - 1.0
    modulus = lam_real * lam_real + frequency * frequency
    ratio_real = (minus_real * lam_real + bar_imag * frequency) / modulus
    ratio_imag = (bar_imag * lam_real - minus_real * frequency) / modulus
    in_real = b_in[..., :entries]
    in_imag = b_in[..., entries:]
    input_matrix_real = ratio_real[:, None, :] * in_real - ratio_imag[:, None, :] * in_imag
    input_matrix_imag = ratio_real[:, None, :] * in_imag + ratio_imag[:, None, :] * in_real
    forcing_real = jnp.einsum(
        "rxf,xfb->rxb", input_rows, input_matrix_real, precision=top_precision
    )
    forcing_imag = jnp.einsum(
        "rxf,xfb->rxb", input_rows, input_matrix_imag, precision=top_precision
    )
    old_real = state[..., :entries]
    old_imag = state[..., entries:]
    following_real = bar_real * old_real - bar_imag * old_imag + forcing_real
    following_imag = bar_real * old_imag + bar_imag * old_real + forcing_imag
    output_real = c_out[..., :entries]
    output_imag = c_out[..., entries:]
    output_matrix = jnp.einsum("lzt,zft->lzf", following_real, output_real, precision=top_precision)
    output_matrix = output_matrix - jnp.einsum(
        "lzt,zft->lzf", following_imag, output_imag, precision=top_precision
    )
    output_matrix = output_matrix + skip.reshape(group_count, width) * input_rows
    activated = jax.nn.gelu(output_matrix).reshape(seq_count, group_count * width)
    return (activated, jnp.concatenate([following_real, following_imag], axis=-1))


def route_weights(normed, routes, w_group, w_expert):
    group_total = w_group.shape[1]
    expert_total = w_expert.shape[1]
    per_group = expert_total // group_total
    group_logit = jnp.dot(normed, w_group, preferred_element_type=jnp.float32)
    group_exp = jnp.exp(group_logit)
    group_prob = group_exp / jnp.sum(group_exp, -1, keepdims=True)
    chosen = routes[:, 0] // per_group
    group_pick = jnp.sum(
        jnp.where(
            chosen[:, None] == jnp.arange(group_total, dtype=jnp.int32)[None, :], group_prob, 0.0
        ),
        -1,
    )
    expert_logit = jnp.dot(normed, w_expert, preferred_element_type=jnp.float32)
    picked = jnp.sum(
        jnp.where(
            routes[:, :, None] == jnp.arange(expert_total, dtype=jnp.int32)[None, None, :],
            expert_logit[:, None, :],
            0.0,
        ),
        -1,
    )
    pair_exp = jnp.exp(picked)
    return pair_exp / jnp.sum(pair_exp, -1, keepdims=True) * group_pick[:, None]


def per_device(
    x_in,
    state,
    routes,
    w_in,
    decay_rate,
    frequency,
    log_step,
    b_in,
    c_out,
    skip,
    w_out,
    gain_mix,
    w_group,
    w_expert,
    w_gate,
    w_up,
    w_down,
    gain_moe,
):
    top_precision = lax.Precision.DEFAULT
    seq_count = x_in.shape[0]
    model_width = x_in.shape[1]
    mix_input = jnp.dot(x_in, w_in, preferred_element_type=jnp.float32).astype(jnp.bfloat16)
    activated, new_state = s5_advance(
        mix_input, state, decay_rate, frequency, log_step, b_in, c_out, skip
    )
    partial_mix = jnp.dot(activated.astype(jnp.bfloat16), w_out, preferred_element_type=jnp.float32)
    mixed = taken_together(partial_mix.astype(jnp.bfloat16), "tp").astype(jnp.float32)
    hidden_state = normalize(residual_scale * x_in.astype(jnp.float32) + mixed, gain_mix)
    hidden_bf = hidden_state.astype(jnp.bfloat16)
    route_weight = route_weights(hidden_bf, routes, w_group, w_expert)
    expert_total = w_expert.shape[1]
    ep_count = lax.axis_size("ep")
    local_experts = w_gate.shape[0]
    capacity = max(2, 4 * seq_count // expert_total)
    total_slots = expert_total * capacity
    hits = (routes[:, :, None] == jnp.arange(expert_total, dtype=jnp.int32)[None, None, :]).astype(
        jnp.int32
    )
    tally = jnp.sum(hits, axis=1)
    prior = jnp.cumsum(tally, axis=0) - tally
    slot_in_block = jnp.sum(prior[:, None, :] * hits, axis=-1)
    target = routes * capacity + slot_in_block
    slot_ids = jnp.arange(total_slots, dtype=jnp.int32)
    matches = target[:, :, None] == slot_ids[None, None, :]
    dispatch_map = jnp.any(slot_ids[:, None, None] == target[None, :, :], axis=-1).astype(
        jnp.bfloat16
    )
    combine_map = jnp.sum(jnp.where(matches, route_weight[:, :, None], 0.0), axis=1)
    buffer = jnp.dot(dispatch_map, hidden_bf, preferred_element_type=jnp.float32).astype(
        jnp.bfloat16
    )
    buffer = buffer.reshape(ep_count, local_experts, capacity, model_width)
    column_width = model_width // lax.axis_size("tp")
    own_columns = lax.dynamic_slice_in_dim(
        buffer, lax.axis_index("tp") * column_width, column_width, 3
    )
    piece = gather_directly(
        lax.all_to_all(own_columns, "ep", split_axis=0, concat_axis=0, tiled=True), "tp", 3
    )
    gate_part = jnp.einsum("njcd,jdf->njcf", piece, w_gate, preferred_element_type=jnp.float32)
    up_part = jnp.einsum("njcd,jdf->njcf", piece, w_up, preferred_element_type=jnp.float32)
    act = (jax.nn.silu(gate_part) * up_part).astype(jnp.bfloat16)
    share = sent_and_summed(
        jnp.einsum("njcf,jfd->njcd", act, w_down, preferred_element_type=jnp.float32).astype(
            jnp.bfloat16
        ),
        "tp",
        3,
    ).astype(jnp.bfloat16)
    returned_rows = lax.all_to_all(share, "ep", split_axis=0, concat_axis=0, tiled=True)
    flat_rows = returned_rows.reshape(total_slots, returned_rows.shape[3])
    moe = jnp.dot(
        combine_map,
        lax.all_gather(flat_rows, "tp", axis=1, tiled=True).astype(jnp.float32),
        precision=top_precision,
    )
    layer_out = normalize(residual_scale * hidden_state + moe, gain_moe).astype(jnp.bfloat16)
    return (layer_out, new_state)


def solution(mesh):
    in_specs = (
        P(("grp", "ep"), None),
        P(("grp", "ep"), "tp", None),
        P(("grp", "ep"), None),
        P(None, "tp"),
        P("tp", None),
        P("tp", None),
        P("tp"),
        P("tp", None, None),
        P("tp", None, None),
        P("tp"),
        P("tp", None),
        P(),
        P(),
        P(),
        P("ep", None, "tp"),
        P("ep", None, "tp"),
        P("ep", "tp", None),
        P(),
    )
    out_specs = (P(("grp", "ep"), None), P(("grp", "ep"), "tp", None))
    return jax.shard_map(
        per_device, mesh=mesh, in_specs=in_specs, out_specs=out_specs, check_vma=False
    )
```

profile of v0, /device:TPU:40, one launch (start us, length us, event | category | flops | bytes accessed | tf_op | source)
XLA Modules:
  0.0 197.4 jit_solution(56538877208457532)
XLA Ops:
  7.2 0.8 exp.20
  8.0 1.9 convolution_convert_fusion.3
  10.9 0.5 fusion.5
  11.4 1.4 fusion.6
  12.9 1.6 fusion.41
  15.3 1.2 broadcast_in_dim.24
  16.4 4.6 %all-to-all-start = ((bf16[4,64,2048]{2,1,0:T(8,128)(2,1)}), bf16[4,64,2048]{2,1,0:T(8,128)(2,1)}, u32[]{:S(2)}, u32[]{:S(2)}) async-start(bf16[4,64,2048]{2,1,0:T(8,128)(2,1)} %broadcast_in_dim.24), calls=%async_computation | async-start | bytes 2097152 | tf_op jit(solution)/shard_map/all_to_all | solution.py:12
  21.5 14.8 %all-to-all-done = bf16[4,64,2048]{2,1,0:T(8,128)(2,1)} async-done(((bf16[4,64,2048]{2,1,0:T(8,128)(2,1)}), bf16[4,64,2048]{2,1,0:T(8,128)(2,1)}, u32[]{:S(2)}, u32[]{:S(2)}) %all-to-all-start) | async-done | bytes 1048608 | tf_op jit(solution)/shard_map/all_to_all | solution.py:12
  36.3 1.4 convert_reduce_fusion
  37.7 1.1 fusion.59
  38.8 1.2 multiply_reduce_fusion.1
  40.0 1.1 fusion.23
  41.2 0.7 copy-done.3
  41.8 1.5 convolution_convert_fusion.1
  43.3 2.3 %reshape.109 = bf16[32,2,4,2048]{3,2,1,0:T(4,128)(2,1)} reshape(bf16[256,2048]{1,0:T(8,128)(2,1)} %convolution_convert_fusion.1) | data formatting | bytes 2097152 | tf_op jit(solution)/shard_map/reshape | solution.py:170
  45.6 1.0 constant_dynamic-slice_fusion
  46.6 46.5 %all_to_all.25 = bf16[32,2,4,512]{3,2,1,0:T(4,128)(2,1)S(1)} all-to-all(bf16[32,2,4,512]{3,2,1,0:T(4,128)(2,1)S(1)} %constant_dynamic-slice_fusion), channel_id=1, replica_groups=mesh['grp'=2,'ep'=32,'tp'=4] {'ep'}, dimensions={0} | all-to-all | bytes 524288 | tf_op jit(solution)/shard_map/all_to_all | solution.py:176
  93.4 18.0 %all_to_all.26 = bf16[4,32,2,4,512]{4,1,3,2,0:T(8,128)(2,1)S(1)} all-to-all(bf16[4,32,2,4,512]{4,1,3,2,0:T(8,128)(2,1)S(1)} %broadcast_in_dim.34), channel_id=1, replica_groups=mesh['grp'=2,'ep'=32,'tp'=4] {'tp'}, dimensions={0} | all-to-all | bytes 2097152 | tf_op jit(solution)/shard_map/all_to_all | solution.py:12
  111.6 1.0 copy-done.1
  112.6 1.2 fusion.7
  113.7 3.8 %convolution_convert_fusion = bf16[2,32,4,2048]{3,1,2,0:T(8,128)(2,1)} fusion(bf16[2,256,2048]{2,1,0:T(8,128)(2,1)S(1)} %copy-done, bf16[32,2,4,2048]{3,0,2,1:T(8,128)(2,1)} %bitcast.85, bf16[2,2048,256]{2,1,0:T(8,128)(2,1)} %param.33, f32[32,2,4,256]{3,0,2,1:T(8,128)} %fusion.7), kind=kOutput, calls=%fused_computation | convolution fusion | flops 537788416 | bytes 6553600 | tf_op jit(solution)/shard_map/njcf,jfd->njcd/dot_general | solution.py:182
  117.5 1.4 copy.95
  118.8 17.5 %all_to_all.27 = bf16[4,32,2,4,512]{4,1,3,2,0:T(8,128)(2,1)} all-to-all(bf16[4,32,2,4,512]{4,1,3,2,0:T(8,128)(2,1)S(1)} %bitcast.88), channel_id=1, replica_groups=mesh['grp'=2,'ep'=32,'tp'=4] {'tp'}, dimensions={0} | all-to-all | bytes 2097152 | tf_op jit(solution)/shard_map/all_to_all | solution.py:38
  136.3 2.2 %reduce_sum.130 = bf16[32,2,4,512]{3,0,2,1:T(8,128)(2,1)} reduce(bf16[4,32,2,4,512]{4,1,3,2,0:T(8,128)(2,1)} %all_to_all.27, bf16[]{:T(256)} %constant.58.clone.1), dimensions={0}, to_apply=%region_12.13 | reduce | flops 393216 | bytes 1310722 | tf_op jit(solution)/shard_map/reduce_sum | solution.py:39
  138.5 1.2 copy.80
  139.7 26.5 %all_to_all.28 = bf16[32,2,4,512]{3,2,1,0:T(4,128)(2,1)} all-to-all(bf16[32,2,4,512]{3,2,1,0:T(4,128)(2,1)S(1)} %copy.80), channel_id=1, replica_groups=mesh['grp'=2,'ep'=32,'tp'=4] {'ep'}, dimensions={0} | all-to-all | bytes 524288 | tf_op jit(solution)/shard_map/all_to_all | solution.py:188
  166.2 1.7 reshape.112
  168.0 1.5 pad_maximum_fusion
  169.5 1.3 copy.81
  171.7 16.1 %all-gather.2.cloned.1.call-done = bf16[256,2048]{1,0:T(8,128)(2,1)} async-done(((bf16[256,512]{1,0:T(8,128)(2,1)}), bf16[256,2048]{1,0:T(8,128)(2,1)}) %all-gather.2.cloned.1.call-update) | async-done | bytes 1048592 | tf_op jit(solution)/shard_map/all_gather | solution.py:192
  187.8 1.7 fusion.62
  189.7 0.8 multiply_convert_fusion
  (64 shorter events, 3.7 us)
Async XLA Ops:
  7.2 106.6 %copy-start = (bf16[2,256,2048]{2,1,0:T(8,128)(2,1)S(1)}, bf16[2,256,2048]{2,1,0:T(8,128)(2,1)}, u32[]{:S(2)}) copy-start(bf16[2,256,2048]{2,1,0:T(8,128)(2,1)} %param.34) | copy-start | bytes 6291460
  7.2 2.9 %copy-start.5 = (f32[64,24,128]{2,1,0:T(8,128)S(1)}, f32[64,24,128]{2,1,0:T(8,128)}, u32[]{:S(2)}) copy-start(f32[64,24,128]{2,1,0:T(8,128)} %param.19) | copy-start | bytes 2359300
  9.9 0.7 copy-start.14
  9.9 0.7 copy-start.15
  9.9 0.9 copy-start.9
  10.9 1.9 copy-start.17
  10.9 2.0 %copy-start.8 = (f32[24,16,128]{2,1,0:T(8,128)S(1)}, f32[24,16,128]{2,1,0:T(8,128)}, u32[]{:S(2)}) copy-start(f32[24,16,128]{2,1,0:T(8,128)} %param.26) | copy-start | bytes 589828
  12.9 2.0 %copy-start.7 = (bf16[384,2048]{1,0:T(8,128)(2,1)S(1)}, bf16[384,2048]{1,0:T(8,128)(2,1)}, u32[]{:S(2)}) copy-start(bf16[384,2048]{1,0:T(8,128)(2,1)} %param.28) | copy-start | bytes 4718596
  15.3 5.8 %copy-start.13 = (s32[64,2]{0,1:T(2,128)S(1)}, s32[64,2]{0,1:T(2,128)}, u32[]{:S(2)}) copy-start(s32[64,2]{0,1:T(2,128)} %param.20) | copy-start | bytes 1540
  16.4 19.8 %all-to-all-start = ((bf16[4,64,2048]{2,1,0:T(8,128)(2,1)}), bf16[4,64,2048]{2,1,0:T(8,128)(2,1)}, u32[]{:S(2)}, u32[]{:S(2)}) async-start(bf16[4,64,2048]{2,1,0:T(8,128)(2,1)} %broadcast_in_dim.24), calls=%async_computation | async-start | bytes 2097152 | tf_op jit(solution)/shard_map/all_to_all | solution.py:12
  21.0 19.0 %copy-start.11 = (f32[2048]{0:T(1024)S(1)}, f32[2048]{0:T(1024)}, u32[]{:S(2)}) copy-start(f32[2048]{0:T(1024)} %param.29) | copy-start | bytes 24580
  21.0 166.7 %all-gather.2.cloned.1.call-start = ((), (), s32[]{:S(2)}) async-start(), calls=%async_computation.5 | async-start | bytes 1310720 | tf_op jit(solution)/shard_map/all_gather | solution.py:192
  41.1 0.7 copy-start.3
  93.4 19.2 %copy-start.6 = (bf16[2,2048,256]{2,1,0:T(8,128)(2,1)S(1)}, bf16[2,2048,256]{2,1,0:T(8,128)(2,1)}, u32[]{:S(2)}) copy-start(bf16[2,2048,256]{2,1,0:T(8,128)(2,1)} %param.32) | copy-start | bytes 6291460
  111.6 1.0 copy-start.1
  168.0 2.9 %copy-start.4 = (bf16[64,2048]{1,0:T(8,128)(2,1)S(1)}, bf16[64,2048]{1,0:T(8,128)(2,1)}, u32[]{:S(2)}) copy-start(bf16[64,2048]{1,0:T(8,128)(2,1)} %copy-done.3) | copy-start | bytes 786436
  168.0 2.9 %copy-start.10 = (bf16[2048,64]{0,1:T(8,128)(2,1)S(1)}, bf16[2048,64]{0,1:T(8,128)(2,1)}, u32[]{:S(2)}) copy-start(bf16[2048,64]{0,1:T(8,128)(2,1)} %param.31) | copy-start | bytes 786436
  168.0 3.3 %copy-start.12 = (bf16[2048,4]{0,1:T(4,128)(2,1)S(1)}, bf16[2048,4]{0,1:T(4,128)(2,1)}, u32[]{:S(2)}) copy-start(bf16[2048,4]{0,1:T(4,128)(2,1)} %param.30) | copy-start | bytes 49156
  169.5 18.3 %copy-start.2 = (bf16[64,2048]{1,0:T(8,128)(2,1)S(1)}, bf16[64,2048]{1,0:T(8,128)(2,1)}, u32[]{:S(2)}) copy-start(bf16[64,2048]{1,0:T(8,128)(2,1)} %param.18) | copy-start | bytes 786436
  170.8 18.8 %copy-start.16 = (f32[2048]{0:T(1024)S(1)}, f32[2048]{0:T(1024)}, u32[]{:S(2)}) copy-start(f32[2048]{0:T(1024)} %param.35) | copy-start | bytes 24580
Sparse Core Ops, SparseCore 0:
  168.1 19.5 all-gather.1
where the time goes:
time: 198 us; the launch traced here: 197 us
  blocking collectives  109 us (55%)
  waiting for transfers between devices  30.9 us (16%)
  matrix products  14.6 us (7%)
  between operations  14.4 us (7%)
  local copies, waits for them, and re-layouts  13.8 us (7%)
  other arithmetic  10.5 us (5%)
  starting transfers between devices  4.58 us (2%)
    all_to_all x1, blocking collectives, per_device(): lax.all_to_all(own_columns, 'ep', split_axis=0, concat_axis=0, tiled=True)  46.5 us
    all_to_all x1, blocking collectives, per_device(): lax.all_to_all(share, 'ep', split_axis=0, concat_axis=0, tiled=True)  26.5 us
    all_to_all x1, blocking collectives, sent_to_all(): lax.all_to_all(jnp.broadcast_to(x[None], (devices, *x.shape)), axis, 0, 0...  18 us
    all_to_all x1, blocking collectives, sent_and_summed(): parts = lax.all_to_all(split_up(x, dim, devices), axis, 0, 0, tiled=True)  17.5 us
    all_gather x1, waiting for transfers between devices, per_device(): lax.all_gather(flat_rows, 'tp', axis=1, tiled=True).astype(jnp.float32)  16.1 us
    all_to_all x1, waiting for transfers between devices, sent_to_all(): lax.all_to_all(jnp.broadcast_to(x[None], (devices, *x.shape)), axis, 0, 0...  14.8 us
    all_to_all x1, starting transfers between devices, sent_to_all(): lax.all_to_all(jnp.broadcast_to(x[None], (devices, *x.shape)), axis, 0, 0...  4.58 us
  transfers between devices with their start and end apart: 2, of which 2 were waited for; matrix products, arithmetic and copies ran while one was open for 2% of the time, Pallas kernels for 0%

commit v1 on v0

--- a/solution.py
+++ b/solution.py
@@ -189,7 +189,9 @@
     flat_rows = returned_rows.reshape(total_slots, returned_rows.shape[3])
     moe = jnp.dot(
         combine_map,
-        lax.all_gather(flat_rows, "tp", axis=1, tiled=True).astype(jnp.float32),
+        jnp.concatenate(
+            lax.all_to_all(jnp.stack([flat_rows] * lax.axis_size("tp")), "tp", 0, 0), axis=1
+        ).astype(jnp.float32),
         precision=top_precision,
     )
     layer_out = normalize(residual_scale * hidden_state + moe, gain_moe).astype(jnp.bfloat16)

time: 198 us -> 188 us (0.949)
  blocking collectives: 109 us -> 82.1 us
  waiting for transfers between devices: 30.9 us -> 47.7 us
  between operations: 14.4 us -> 0.98 us
  starting transfers between devices: 4.58 us -> 14.3 us
  local copies, waits for them, and re-layouts: 13.8 us -> 16.7 us
    all_to_all x0 -> x2, waiting for transfers between devices: none -> 32.9 us  [the longest x1 18.8 us: per_device(): lax.all_to_all(share, 'ep', split_axis=0, concat_axis=0, tiled=True)]
    all_to_all x1 -> x0, blocking collectives: 26.5 us -> none  [per_device(): lax.all_to_all(share, 'ep', split_axis=0, concat_axis=0, tiled=True)]
    all_gather x1 -> x0, waiting for transfers between devices: 16.1 us -> none  [per_device(): lax.all_gather(flat_rows, 'tp', axis=1, tiled=True).astype(jnp.float32)]
    all_to_all x0 -> x2, starting transfers between devices: none -> 9.72 us  [the longest x1 5.4 us: per_device(): lax.all_to_all(share, 'ep', split_axis=0, concat_axis=0, tiled=True)]
    another operation x0 -> x3, local copies, waits for them, and re-layouts: none -> 3.95 us  [per_device(): jnp.stack([flat_rows] * lax.axis_size('tp'))]
  transfers between devices with their start and end apart: 2 -> 3, of which waited for: 2 -> 3; matrix products, arithmetic and copies ran while one was open for 2% -> 2% of each run, Pallas kernels for 0% -> 0%
where the time goes in v1:
time: 188 us; the launch traced here: 187 us
  blocking collectives  82.1 us (44%)
  waiting for transfers between devices  47.7 us (25%)
  local copies, waits for them, and re-layouts  16.7 us (9%)
  matrix products  14.7 us (8%)
  starting transfers between devices  14.3 us (8%)
  other arithmetic  10.5 us (6%)
    all_to_all x1, blocking collectives, per_device(): lax.all_to_all(own_columns, 'ep', split_axis=0, concat_axis=0, tiled=True)  46.5 us
    all_to_all x1, waiting for transfers between devices, per_device(): lax.all_to_all(share, 'ep', split_axis=0, concat_axis=0, tiled=True)  18.8 us
    all_to_all x1, blocking collectives, sent_to_all(): lax.all_to_all(jnp.broadcast_to(x[None], (devices, *x.shape)), axis, 0, 0...  18 us
    all_to_all x1, blocking collectives, sent_and_summed(): parts = lax.all_to_all(split_up(x, dim, devices), axis, 0, 0, tiled=True)  17.5 us
    all_to_all x1, waiting for transfers between devices, sent_to_all(): lax.all_to_all(jnp.broadcast_to(x[None], (devices, *x.shape)), axis, 0, 0...  14.8 us
    all_to_all x1, waiting for transfers between devices, per_device(): lax.all_to_all(jnp.stack([flat_rows] * lax.axis_size('tp')), 'tp', 0, 0)  14.1 us
    all_to_all x1, starting transfers between devices, per_device(): lax.all_to_all(share, 'ep', split_axis=0, concat_axis=0, tiled=True)  5.4 us
    all_to_all x1, starting transfers between devices, sent_to_all(): lax.all_to_all(jnp.broadcast_to(x[None], (devices, *x.shape)), axis, 0, 0...  4.58 us
  transfers between devices with their start and end apart: 3, of which 3 were waited for; matrix products, arithmetic and copies ran while one was open for 2% of the time, Pallas kernels for 0%

profile of v1, /device:TPU:40, one launch (start us, length us, event | category | flops | bytes accessed | tf_op | source)
XLA Modules:
  0.0 186.9 jit_solution(1396444726638524079)
XLA Ops:
  1.5 1.9 %convolution_convert_fusion.3 = bf16[64,384]{1,0:T(8,128)(2,1)S(1)} fusion(bf16[64,2048]{1,0:T(8,128)(2,1)} %param.18, bf16[2048,384]{1,0:T(8,128)(2,1)} %param.21), kind=kOutput, calls=%fused_computation.21 | convolution fusion | flops 100687872 | bytes 1884160 | tf_op jit(solution)/shard_map/dot_general | solution.py:140
  4.8 1.4 fusion.6
  6.3 1.6 fusion.41
  8.7 1.2 broadcast_in_dim.24
  9.9 4.6 %all-to-all-start = ((bf16[4,64,2048]{2,1,0:T(8,128)(2,1)}), bf16[4,64,2048]{2,1,0:T(8,128)(2,1)}, u32[]{:S(2)}, u32[]{:S(2)}) async-start(bf16[4,64,2048]{2,1,0:T(8,128)(2,1)} %broadcast_in_dim.24), calls=%async_computation | async-start | bytes 2097152 | tf_op jit(solution)/shard_map/all_to_all | solution.py:12
  14.9 14.8 %all-to-all-done = bf16[4,64,2048]{2,1,0:T(8,128)(2,1)} async-done(((bf16[4,64,2048]{2,1,0:T(8,128)(2,1)}), bf16[4,64,2048]{2,1,0:T(8,128)(2,1)}, u32[]{:S(2)}, u32[]{:S(2)}) %all-to-all-start) | async-done | bytes 1048608 | tf_op jit(solution)/shard_map/all_to_all | solution.py:12
  29.7 1.4 convert_reduce_fusion
  31.2 1.1 fusion.59
  32.3 1.2 multiply_reduce_fusion.1
  33.5 1.1 fusion.23
  35.3 1.5 convolution_convert_fusion.1
  36.8 2.3 %reshape.114 = bf16[32,2,4,2048]{3,2,1,0:T(4,128)(2,1)} reshape(bf16[256,2048]{1,0:T(8,128)(2,1)} %convolution_convert_fusion.1) | data formatting | bytes 2097152 | tf_op jit(solution)/shard_map/reshape | solution.py:170
  39.0 1.0 constant_dynamic-slice_fusion
  40.1 46.5 %all_to_all.30 = bf16[32,2,4,512]{3,2,1,0:T(4,128)(2,1)S(1)} all-to-all(bf16[32,2,4,512]{3,2,1,0:T(4,128)(2,1)S(1)} %constant_dynamic-slice_fusion), channel_id=1, replica_groups=mesh['grp'=2,'ep'=32,'tp'=4] {'ep'}, dimensions={0} | all-to-all | bytes 524288 | tf_op jit(solution)/shard_map/all_to_all | solution.py:176
  86.8 18.0 %all_to_all.31 = bf16[4,32,2,4,512]{4,1,3,2,0:T(8,128)(2,1)S(1)} all-to-all(bf16[4,32,2,4,512]{4,1,3,2,0:T(8,128)(2,1)S(1)} %broadcast_in_dim.34), channel_id=1, replica_groups=mesh['grp'=2,'ep'=32,'tp'=4] {'tp'}, dimensions={0} | all-to-all | bytes 2097152 | tf_op jit(solution)/shard_map/all_to_all | solution.py:12
  105.0 1.0 copy-done.1
  106.0 1.2 fusion.7
  107.2 3.8 %convolution_convert_fusion = bf16[2,32,4,2048]{3,1,2,0:T(8,128)(2,1)} fusion(bf16[2,256,2048]{2,1,0:T(8,128)(2,1)S(1)} %copy-done, bf16[32,2,4,2048]{3,0,2,1:T(8,128)(2,1)} %bitcast.88, bf16[2,2048,256]{2,1,0:T(8,128)(2,1)} %param.33, f32[32,2,4,256]{3,0,2,1:T(8,128)} %fusion.7), kind=kOutput, calls=%fused_computation | convolution fusion | flops 537788416 | bytes 6553600 | tf_op jit(solution)/shard_map/njcf,jfd->njcd/dot_general | solution.py:182
  110.9 1.4 copy.96
  112.3 17.5 %all_to_all.32 = bf16[4,32,2,4,512]{4,1,3,2,0:T(8,128)(2,1)} all-to-all(bf16[4,32,2,4,512]{4,1,3,2,0:T(8,128)(2,1)S(1)} %bitcast.91), channel_id=1, replica_groups=mesh['grp'=2,'ep'=32,'tp'=4] {'tp'}, dimensions={0} | all-to-all | bytes 2097152 | tf_op jit(solution)/shard_map/all_to_all | solution.py:38
  129.8 2.2 %reduce_sum.130 = bf16[32,2,4,512]{3,0,2,1:T(8,128)(2,1)} reduce(bf16[4,32,2,4,512]{4,1,3,2,0:T(8,128)(2,1)} %all_to_all.32, bf16[]{:T(256)} %constant.58.clone.1), dimensions={0}, to_apply=%region_12.13 | reduce | flops 393216 | bytes 1310722 | tf_op jit(solution)/shard_map/reduce_sum | solution.py:39
  132.0 1.9 copy.80
  133.8 5.4 %all-to-all-start.4 = ((bf16[32,2,4,512]{3,2,1,0:T(4,128)(2,1)}), bf16[32,2,4,512]{3,2,1,0:T(4,128)(2,1)}, u32[]{:S(2)}, u32[]{:S(2)}) async-start(bf16[32,2,4,512]{3,2,1,0:T(4,128)(2,1)} %copy.80), calls=%async_computation.4 | async-start | bytes 524288 | tf_op jit(solution)/shard_map/all_to_all | solution.py:188
  139.2 1.5 pad_maximum_fusion
  140.7 1.3 copy.82
  142.5 18.8 %all-to-all-done.4 = bf16[32,2,4,512]{3,2,1,0:T(4,128)(2,1)} async-done(((bf16[32,2,4,512]{3,2,1,0:T(4,128)(2,1)}), bf16[32,2,4,512]{3,2,1,0:T(4,128)(2,1)}, u32[]{:S(2)}, u32[]{:S(2)}) %all-to-all-start.4) | async-done | bytes 262176 | tf_op jit(solution)/shard_map/all_to_all | solution.py:188
  161.3 1.7 stack_reshape.2
  163.0 1.1 copy.81
  164.1 1.1 stack.3
  165.2 4.3 %all-to-all-start.5 = ((bf16[4,256,512]{1,2,0:T(8,128)(2,1)}), bf16[4,256,512]{1,2,0:T(8,128)(2,1)}, u32[]{:S(2)}, u32[]{:S(2)}) async-start(bf16[4,256,512]{1,2,0:T(8,128)(2,1)} %stack.3), calls=%async_computation.5 | async-start | bytes 2097152 | tf_op jit(solution)/shard_map/all_to_all | solution.py:193
  170.0 14.1 %all-to-all-done.5 = bf16[4,256,512]{1,2,0:T(8,128)(2,1)} async-done(((bf16[4,256,512]{1,2,0:T(8,128)(2,1)}), bf16[4,256,512]{1,2,0:T(8,128)(2,1)}, u32[]{:S(2)}, u32[]{:S(2)}) %all-to-all-start.5) | async-done | bytes 1048608 | tf_op jit(solution)/shard_map/all_to_all | solution.py:193
  184.1 1.8 fusion.62
  (68 shorter events, 6.5 us)
Async XLA Ops:
  0.6 106.6 %copy-start = (bf16[2,256,2048]{2,1,0:T(8,128)(2,1)S(1)}, bf16[2,256,2048]{2,1,0:T(8,128)(2,1)}, u32[]{:S(2)}) copy-start(bf16[2,256,2048]{2,1,0:T(8,128)(2,1)} %param.34) | copy-start | bytes 6291460
  0.6 2.9 %copy-start.6 = (f32[64,24,128]{2,1,0:T(8,128)S(1)}, f32[64,24,128]{2,1,0:T(8,128)}, u32[]{:S(2)}) copy-start(f32[64,24,128]{2,1,0:T(8,128)} %param.19) | copy-start | bytes 2359300
  3.4 0.7 copy-start.15
  3.4 0.7 copy-start.16
  3.4 0.9 copy-start.10
  4.3 1.9 %copy-start.18 = (f32[384]{0:T(512)S(1)}, f32[384]{0:T(512)}, u32[]{:S(2)}) copy-start(f32[384]{0:T(512)} %param.27) | copy-start | bytes 4612
  4.3 2.0 %copy-start.9 = (f32[24,16,128]{2,1,0:T(8,128)S(1)}, f32[24,16,128]{2,1,0:T(8,128)}, u32[]{:S(2)}) copy-start(f32[24,16,128]{2,1,0:T(8,128)} %param.26) | copy-start | bytes 589828
  6.3 2.0 %copy-start.8 = (bf16[384,2048]{1,0:T(8,128)(2,1)S(1)}, bf16[384,2048]{1,0:T(8,128)(2,1)}, u32[]{:S(2)}) copy-start(bf16[384,2048]{1,0:T(8,128)(2,1)} %param.28) | copy-start | bytes 4718596
  8.7 5.8 %copy-start.14 = (s32[64,2]{0,1:T(2,128)S(1)}, s32[64,2]{0,1:T(2,128)}, u32[]{:S(2)}) copy-start(s32[64,2]{0,1:T(2,128)} %param.20) | copy-start | bytes 1540
  9.9 19.8 %all-to-all-start = ((bf16[4,64,2048]{2,1,0:T(8,128)(2,1)}), bf16[4,64,2048]{2,1,0:T(8,128)(2,1)}, u32[]{:S(2)}, u32[]{:S(2)}) async-start(bf16[4,64,2048]{2,1,0:T(8,128)(2,1)} %broadcast_in_dim.24), calls=%async_computation | async-start | bytes 2097152 | tf_op jit(solution)/shard_map/all_to_all | solution.py:12
  14.5 19.0 %copy-start.12 = (f32[2048]{0:T(1024)S(1)}, f32[2048]{0:T(1024)}, u32[]{:S(2)}) copy-start(f32[2048]{0:T(1024)} %param.29) | copy-start | bytes 24580
  34.6 0.7 copy-start.3
  86.8 19.2 %copy-start.7 = (bf16[2,2048,256]{2,1,0:T(8,128)(2,1)S(1)}, bf16[2,2048,256]{2,1,0:T(8,128)(2,1)}, u32[]{:S(2)}) copy-start(bf16[2,2048,256]{2,1,0:T(8,128)(2,1)} %param.32) | copy-start | bytes 6291460
  105.0 1.0 copy-start.1
  133.8 27.4 %all-to-all-start.4 = ((bf16[32,2,4,512]{3,2,1,0:T(4,128)(2,1)}), bf16[32,2,4,512]{3,2,1,0:T(4,128)(2,1)}, u32[]{:S(2)}, u32[]{:S(2)}) async-start(bf16[32,2,4,512]{3,2,1,0:T(4,128)(2,1)} %copy.80), calls=%async_computation.4 | async-start | bytes 524288 | tf_op jit(solution)/shard_map/all_to_all | solution.py:188
  139.2 2.8 %copy-start.4 = (bf16[64,2048]{1,0:T(8,128)(2,1)S(1)}, bf16[64,2048]{1,0:T(8,128)(2,1)}, u32[]{:S(2)}) copy-start(bf16[64,2048]{1,0:T(8,128)(2,1)} %copy-done.3) | copy-start | bytes 786436
  139.2 2.8 %copy-start.11 = (bf16[2048,64]{0,1:T(8,128)(2,1)S(1)}, bf16[2048,64]{0,1:T(8,128)(2,1)}, u32[]{:S(2)}) copy-start(bf16[2048,64]{0,1:T(8,128)(2,1)} %param.31) | copy-start | bytes 786436
  163.0 6.6 %copy-start.5 = (bf16[64,2048]{1,0:T(8,128)(2,1)S(1)}, bf16[64,2048]{1,0:T(8,128)(2,1)}, u32[]{:S(2)}) copy-start(bf16[64,2048]{1,0:T(8,128)(2,1)} %copy-done.3) | copy-start | bytes 786436
  163.0 6.6 %copy-start.13 = (bf16[2048,4]{0,1:T(4,128)(2,1)S(1)}, bf16[2048,4]{0,1:T(4,128)(2,1)}, u32[]{:S(2)}) copy-start(bf16[2048,4]{0,1:T(4,128)(2,1)} %param.30) | copy-start | bytes 49156
  163.0 21.1 %copy-start.2 = (bf16[64,2048]{1,0:T(8,128)(2,1)S(1)}, bf16[64,2048]{1,0:T(8,128)(2,1)}, u32[]{:S(2)}) copy-start(bf16[64,2048]{1,0:T(8,128)(2,1)} %param.18) | copy-start | bytes 786436
  165.2 18.8 %all-to-all-start.5 = ((bf16[4,256,512]{1,2,0:T(8,128)(2,1)}), bf16[4,256,512]{1,2,0:T(8,128)(2,1)}, u32[]{:S(2)}, u32[]{:S(2)}) async-start(bf16[4,256,512]{1,2,0:T(8,128)(2,1)} %stack.3), calls=%async_computation.5 | async-start | bytes 2097152 | tf_op jit(solution)/shard_map/all_to_all | solution.py:193
  169.6 16.5 %copy-start.17 = (f32[2048]{0:T(1024)S(1)}, f32[2048]{0:T(1024)}, u32[]{:S(2)}) copy-start(f32[2048]{0:T(1024)} %param.35) | copy-start | bytes 24580
